TPU v7x, 256 devices: a whole 4x4x8 slice. The times are simulated.
256 devices in a mesh: ep: 32 (over z, x), tp: 8 (over y, core).
Axes of the slice: x: 4, y: 4, z: 8, core: 2. Of those that a mesh axis runs over, the one named last changes fastest.
Arguments:
- tokens: bfloat16 [512, 2048], P('ep'), may hold values from -6 to 6
- lengths: int32 [512], P('ep'), may hold values from 1024 to 16384
- old_state: float32 [512, 8, 128, 128], P('ep', 'tp'), may hold values from -2 to 2
- query_weight: bfloat16 [2048, 1024], P(None, 'tp'), may hold values from -0.125 to 0.125
- key_weight: bfloat16 [2048, 1024], P(None, 'tp'), may hold values from -0.125 to 0.125
- value_weight: bfloat16 [2048, 1024], P(None, 'tp'), may hold values from -0.125 to 0.125
- gate_weight: bfloat16 [2048, 1024], P(None, 'tp'), may hold values from -0.125 to 0.125
- head_gain: float32 [1024], P('tp'), may hold values from 0.1 to 1.9
- output_weight: bfloat16 [1024, 2048], P('tp'), may hold values from -0.1875 to 0.1875
- first_gain: float32 [2048], replicated, may hold values from 0.1 to 1.9
- expert_ids: int32 [512, 6], P('ep'), may hold values from 0 to 63, all different within a row; in each aligned block of 16 rows (0 to 15, 16 to 31, ...) at most 2 rows name the same one
- expert_weights: float32 [512, 6], P('ep'), may hold values from 0.05 to 0.8
- expert_gate: bfloat16 [64, 2048, 512], P('ep', None, 'tp'), may hold values from -0.125 to 0.125
- expert_up: bfloat16 [64, 2048, 512], P('ep', None, 'tp'), may hold values from -0.125 to 0.125
- expert_down: bfloat16 [64, 512, 2048], P('ep', 'tp'), may hold values from -0.25 to 0.25
- shared_gate: bfloat16 [2048, 512], P(None, 'tp'), may hold values from -0.125 to 0.125
- shared_up: bfloat16 [2048, 512], P(None, 'tp'), may hold values from -0.125 to 0.125
- shared_down: bfloat16 [512, 2048], P('tp'), may hold values from -0.25 to 0.25
- side_gate: bfloat16 [2048], replicated, may hold values from -0.125 to 0.125
- dense_gate: bfloat16 [2048, 8192], P(None, ('ep', 'tp')), may hold values from -0.125 to 0.125
- dense_up: bfloat16 [2048, 8192], P(None, ('ep', 'tp')), may hold values from -0.125 to 0.125
- dense_down: bfloat16 [8192, 2048], P(('ep', 'tp')), may hold values from -0.25 to 0.25
- second_gain: float32 [2048], replicated, may hold values from 0.1 to 1.9
Outputs:
- layer_out: bfloat16 [512, 2048], P('ep')
- new_state: float32 [512, 8, 128, 128], P('ep', 'tp')
Inputs may be any that keep to these rules, and one draw needn't show every extreme that they name: `expert_ids`: each row names 6 different experts. Among the 16 rows of one index of ep no expert is named by more than 2 rows, a bound that some block reaches.
All inputs are finite; a program needn't handle non-finite values.
Results may differ from a plain program's by a relative error of at most 0.017.
Values may be sent and summed in bfloat16 or wider, within the bound.
A program may use at most 64 MiB of HBM per device.

v0:
```python
import jax
import jax.numpy as jnp
from jax import lax
from jax.sharding import Mesh
from jax.sharding import PartitionSpec as P

HEADS = 8
EP = ("ep_0", "ep_1")
EP_TP = ("ep_0", "ep_1", "tp")


NORM_EPS = 1e-05
RESIDUAL_SCALE = 2.0**0.5


def sent_to_all(shard, axis):
    devices = lax.axis_size(axis)
    return lax.all_to_all(
        jnp.broadcast_to(shard[None], (devices, *shard.shape)), axis, 0, 0, tiled=True
    )


def taken_together(shard, axis):
    everything = sent_to_all(shard, axis)
    return jnp.sum(everything.astype(jnp.float32), axis=0)


def gather_axes(shard, axes, dim):
    result = shard
    for number in range(len(axes) - 1, -1, -1):
        result = lax.all_gather(result, axes[number], axis=dim, tiled=True)
    return result


def reduced_to_own(pieces, axes, sequence):
    shape = [lax.axis_size(a) for a in axes]
    pieces = pieces.reshape(*shape, *pieces.shape[1:])
    pieces = pieces.transpose(*sequence, *range(len(axes), pieces.ndim))
    pieces = pieces.reshape(-1, *pieces.shape[len(axes) :])
    for k in sequence:
        pieces = lax.psum_scatter(pieces, axes[k], scatter_dimension=0, tiled=True)
    return pieces[0]


def split_up(shard, dim, devices):
    shape = shard.shape
    pieces = shard.reshape(*shape[:dim], devices, shape[dim] // devices, *shape[dim + 1 :])
    return jnp.moveaxis(pieces, dim, 0)


def summed_rows(shard, axes, sequence, dim):
    devices = lax.axis_size(axes)
    return reduced_to_own(split_up(shard, dim, devices), axes, sequence)


def rotate(inputs, positions):
    half_size = inputs.shape[-1] // 2
    frequency = 1.0 / 10000.0 ** (jnp.arange(half_size, dtype=jnp.float32) * 2.0 / inputs.shape[-1])
    angles = positions.astype(jnp.float32)[:, None] * frequency[None, :]
    cosine = jnp.cos(angles)[:, None, :]
    sine_part = jnp.sin(angles)[:, None, :]
    first_half = inputs[..., :half_size]
    second_half = inputs[..., half_size:]
    return jnp.concatenate(
        [
            first_half * cosine - second_half * sine_part,
            first_half * sine_part + second_half * cosine,
        ],
        axis=-1,
    )


def layer_norm(inputs, scale_gain):
    average = jnp.mean(inputs, axis=-1, keepdims=True)
    centered = inputs - average
    variance = jnp.mean(centered * centered, axis=-1, keepdims=True)
    return centered * lax.rsqrt(variance + NORM_EPS) * scale_gain


def expert_partial(arrived, expert_gate, expert_up, expert_down):
    gate_part = jnp.einsum(
        "secd,edf->secf", arrived, expert_gate, preferred_element_type=jnp.float32
    )
    up_part = jnp.einsum("secd,edf->secf", arrived, expert_up, preferred_element_type=jnp.float32)
    hidden = (jax.nn.silu(gate_part) * up_part).astype(jnp.bfloat16)
    return jnp.einsum("secf,efd->secd", hidden, expert_down, preferred_element_type=jnp.float32)


def route_experts(after_mixer, expert_ids, expert_weights, expert_gate, expert_up, expert_down):
    row_count, model_width = after_mixer.shape
    top_count = expert_ids.shape[1]
    local_experts = expert_gate.shape[0]
    ep_size = lax.axis_size(EP)
    total_experts = local_experts * ep_size
    capacity = max(2, row_count * top_count // total_experts + 1)
    flat_ids = expert_ids.reshape(-1)
    onehot = (flat_ids[:, None] == jnp.arange(total_experts, dtype=jnp.int32)[None, :]).astype(
        jnp.int32
    )
    slot_rank = jnp.sum(onehot * (jnp.cumsum(onehot, axis=0) - 1), axis=1)
    targets = flat_ids * capacity + slot_rank
    placing = (
        jnp.arange(total_experts * capacity, dtype=jnp.int32)[:, None] == targets[None, :]
    ).astype(jnp.bfloat16)
    repeated = jnp.repeat(after_mixer, top_count, axis=0)
    outgoing = jnp.dot(placing, repeated, preferred_element_type=jnp.float32).astype(jnp.bfloat16)
    outgoing = outgoing.reshape(ep_size, local_experts, capacity, model_width)
    outputs = expert_partial(
        lax.all_to_all(outgoing, EP, split_axis=0, concat_axis=0, tiled=True),
        expert_gate,
        expert_up,
        expert_down,
    )
    summed = (
        taken_together(outputs.astype(jnp.bfloat16), "tp").astype(jnp.float32).astype(jnp.bfloat16)
    )
    returned = lax.all_to_all(summed, EP, split_axis=0, concat_axis=0, tiled=True)
    returned = returned.reshape(total_experts * capacity, model_width)
    gathered_back = jnp.dot(placing.T, returned, preferred_element_type=jnp.float32)
    weighted = gathered_back.reshape(row_count, top_count, model_width) * expert_weights[:, :, None]
    return jnp.sum(weighted, axis=1)


def side_branch(
    after_mixer, shared_gate, shared_up, shared_down, side_gate, dense_gate, dense_up, dense_down
):
    row_count = after_mixer.shape[0]
    row_piece = gather_axes(after_mixer, EP, 0)
    switch = jax.nn.sigmoid(jnp.dot(row_piece, side_gate, preferred_element_type=jnp.float32))
    gate_part = jnp.dot(row_piece, dense_gate, preferred_element_type=jnp.float32)
    up_part = jnp.dot(row_piece, dense_up, preferred_element_type=jnp.float32)
    dense_hidden = (jax.nn.silu(gate_part) * up_part * switch[:, None]).astype(jnp.bfloat16)
    shared_hidden = (
        jax.nn.silu(jnp.dot(after_mixer, shared_gate, preferred_element_type=jnp.float32))
        * jnp.dot(after_mixer, shared_up, preferred_element_type=jnp.float32)
    ).astype(jnp.bfloat16)
    total_rows = dense_hidden.shape[0]
    placed = lax.dynamic_update_slice_in_dim(
        jnp.zeros((total_rows, shared_hidden.shape[1]), jnp.bfloat16),
        shared_hidden,
        lax.axis_index(EP) * row_count,
        0,
    )
    hidden_all = jnp.concatenate([dense_hidden, placed], axis=1)
    down_all = jnp.concatenate([dense_down, shared_down], axis=0)
    group_rows = summed_rows(
        jnp.dot(hidden_all, down_all, preferred_element_type=jnp.float32).astype(jnp.bfloat16),
        EP,
        (1, 0),
        0,
    ).astype(jnp.float32)
    return (
        taken_together(group_rows.astype(jnp.bfloat16), "tp")
        .astype(jnp.float32)
        .astype(jnp.bfloat16)
    )


def per_device(
    tokens,
    lengths,
    old_state,
    query_weight,
    key_weight,
    value_weight,
    gate_weight,
    head_gain,
    output_weight,
    first_gain,
    expert_ids,
    expert_weights,
    expert_gate,
    expert_up,
    expert_down,
    shared_gate,
    shared_up,
    shared_down,
    side_gate,
    dense_gate,
    dense_up,
    dense_down,
    second_gain,
):
    row_count = tokens.shape[0]
    local_heads = old_state.shape[1]
    head_size = old_state.shape[-1]
    queries = jnp.dot(tokens, query_weight, preferred_element_type=jnp.float32).reshape(
        row_count, local_heads, head_size
    )
    keys_raw = jnp.dot(tokens, key_weight, preferred_element_type=jnp.float32).reshape(
        row_count, local_heads, head_size
    )
    keys_raw = keys_raw * head_size ** (-0.5)
    values = jnp.dot(tokens, value_weight, preferred_element_type=jnp.float32).reshape(
        row_count, local_heads, head_size
    )
    gating = jnp.dot(tokens, gate_weight, preferred_element_type=jnp.float32)
    query_rot = rotate(queries, lengths)
    key_rot = rotate(keys_raw, lengths)
    head_ids = (
        lax.axis_index("tp") * local_heads + jnp.arange(local_heads, dtype=jnp.int32)
    ).astype(jnp.float32)
    decays = 1.0 - jnp.exp2(-2.0 - 10.0 * head_ids / (HEADS - 1))
    new_state = (
        decays[None, :, None, None] * old_state + key_rot[:, :, :, None] * values[:, :, None, :]
    )
    readout = jnp.einsum("thi,thij->thj", query_rot, new_state, precision=lax.Precision.HIGHEST)
    normed = layer_norm(readout, head_gain.reshape(local_heads, head_size))
    mixed = (normed.reshape(row_count, local_heads * head_size) * jax.nn.silu(gating)).astype(
        jnp.bfloat16
    )
    partial_value = jnp.dot(mixed, output_weight, preferred_element_type=jnp.float32)
    branch = taken_together(partial_value.astype(jnp.bfloat16), "tp").astype(jnp.float32)
    after_mixer = layer_norm(
        RESIDUAL_SCALE * tokens.astype(jnp.float32) + branch, first_gain
    ).astype(jnp.bfloat16)
    routed = route_experts(
        after_mixer, expert_ids, expert_weights, expert_gate, expert_up, expert_down
    )
    side = side_branch(
        after_mixer,
        shared_gate,
        shared_up,
        shared_down,
        side_gate,
        dense_gate,
        dense_up,
        dense_down,
    )
    total = RESIDUAL_SCALE * after_mixer.astype(jnp.float32) + routed + side.astype(jnp.float32)
    layer_out = layer_norm(total, second_gain).astype(jnp.bfloat16)
    return (layer_out, new_state)


def solution(mesh):
    finer = Mesh(mesh.devices.reshape(8, 4, mesh.shape["tp"]), ("ep_0", "ep_1", "tp"))
    return jax.shard_map(
        per_device,
        mesh=finer,
        in_specs=(
            P(EP, None),
            P(EP),
            P(EP, "tp", None, None),
            P(None, "tp"),
            P(None, "tp"),
            P(None, "tp"),
            P(None, "tp"),
            P("tp"),
            P("tp", None),
            P(),
            P(EP, None),
            P(EP, None),
            P(EP, None, "tp"),
            P(EP, None, "tp"),
            P(EP, "tp", None),
            P(None, "tp"),
            P(None, "tp"),
            P("tp", None),
            P(),
            P(None, EP_TP),
            P(None, EP_TP),
            P(EP_TP, None),
            P(),
        ),
        out_specs=(P(EP, None), P(EP, "tp", None, None)),
        check_vma=False,
    )
```

profile of v0, /device:TPU:1, one launch (start us, length us, event | category | flops | bytes accessed | tf_op | source)
XLA Modules:
  0.0 209.7 jit_solution(6819743417170495981)
XLA Ops:
  7.3 1.4 convolution_bitcast_fusion.2
  8.6 1.3 fusion.6
  10.7 1.3 fusion.56
  12.6 1.0 fusion.9
  13.9 1.4 convolution_convert_fusion.3
  15.4 15.1 %all_to_all.25 = bf16[8,16,2048]{2,1,0:T(8,128)(2,1)S(1)} all-to-all(bf16[8,16,2048]{2,1,0:T(8,128)(2,1)S(1)} %broadcast_in_dim.12), channel_id=1, replica_groups=mesh['ep_0'=8,'ep_1'=4,'tp'=8] {'tp'}, dimensions={0} | all-to-all | bytes 1048576 | tf_op jit(solution)/shard_map/all_to_all | solution.py:18
  31.0 10.9 %all_gather.6 = bf16[64,2048]{1,0:T(8,128)(2,1)} all-gather(bf16[16,2048]{1,0:T(8,128)(2,1)S(1)} %multiply_convert_fusion.1), channel_id=1, replica_groups=mesh['ep_0'=8,'ep_1'=4,'tp'=8] {'ep_1'}, dimensions={0}, use_global_device_ids=true | all-gather | bytes 327680 | tf_op jit(solution)/shard_map/all_gather | solution.py:31
  43.2 1.1 reshape.238
  44.3 10.1 %all-to-all-start.1 = ((bf16[32,2,2,2048]{3,2,1,0:T(2,128)(2,1)}), bf16[32,2,2,2048]{3,2,1,0:T(2,128)(2,1)S(1)}, u32[]{:S(2)}, u32[]{:S(2)}) async-start(bf16[32,2,2,2048]{3,2,1,0:T(2,128)(2,1)} %reshape.238), calls=%async_computation.1 | async-start | bytes 1048576 | tf_op jit(solution)/shard_map/all_to_all | solution.py:109
  54.8 36.2 %all-gather.2.cloned.1.call-done = bf16[512,2048]{1,0:T(8,128)(2,1)} async-done(((bf16[64,2048]{1,0:T(8,128)(2,1)}), bf16[512,2048]{1,0:T(8,128)(2,1)}) %all-gather.2.cloned.1.call-update) | async-done | bytes 2097168 | tf_op jit(solution)/shard_map/all_gather | solution.py:31
  91.0 2.4 %fusion.58 = f32[1,512]{1,0:T(1,128)S(1)} fusion(bf16[512,2048]{1,0:T(8,128)(2,1)} %all-gather.2.cloned.1.call-done, bf16[2048,1]{0,1:T(2,128)(2,1)S(1)} %reshape.251), kind=kOutput, calls=%fused_computation.93 | convolution fusion | flops 2097152 | bytes 2103296 | tf_op jit(solution)/shard_map/dot_general | solution.py:129
  95.1 0.8 convolution_convert_fusion
  95.9 1.5 copy.55
  97.4 1.0 copy-done.19
  99.0 0.8 fusion
  99.7 2.5 %broadcast_in_dim.14 = bf16[8,32,2,2,2048]{4,1,3,2,0:T(8,128)(2,1)} broadcast(bf16[32,2,2,2048]{3,0,2,1:T(8,128)(2,1)S(1)} %fusion), dimensions={1,2,3,4} | broadcast | bytes 4718592 | tf_op jit(solution)/shard_map/broadcast_in_dim | solution.py:19
  102.2 7.0 %all-to-all-start.2 = ((bf16[8,32,2,2,2048]{4,1,3,2,0:T(8,128)(2,1)}), bf16[8,32,2,2,2048]{4,1,3,2,0:T(8,128)(2,1)}, u32[]{:S(2)}, u32[]{:S(2)}) async-start(bf16[8,32,2,2,2048]{4,1,3,2,0:T(8,128)(2,1)} %broadcast_in_dim.14), calls=%async_computation.2 | async-start | bytes 8388608 | tf_op jit(solution)/shard_map/all_to_all | solution.py:18
  109.3 19.8 %reduce-scatter.3.cloned.1.call-done = bf16[8,16,2048]{2,1,0:T(8,128)(2,1)} async-done(((bf16[32,16,2048]{2,1,0:T(8,128)(2,1)}), bf16[8,16,2048]{2,1,0:T(8,128)(2,1)}) %reduce-scatter.3.cloned.1.call-update) | async-done | bytes 524304 | tf_op jit(solution)/shard_map/reduce_scatter | solution.py:41
  129.1 29.0 %all-to-all-done.2 = bf16[8,32,2,2,2048]{4,1,3,2,0:T(8,128)(2,1)} async-done(((bf16[8,32,2,2,2048]{4,1,3,2,0:T(8,128)(2,1)}), bf16[8,32,2,2,2048]{4,1,3,2,0:T(8,128)(2,1)}, u32[]{:S(2)}, u32[]{:S(2)}) %all-to-all-start.2) | async-done | bytes 4194336 | tf_op jit(solution)/shard_map/all_to_all | solution.py:18
  158.1 3.0 %reduce_sum.111 = bf16[32,2,2,2048]{3,0,2,1:T(8,128)(2,1)S(1)} reduce(bf16[8,32,2,2,2048]{4,1,3,2,0:T(8,128)(2,1)} %all-to-all-done.2, bf16[]{:T(256)} %constant.78.clone.1), dimensions={0}, to_apply=%region_7.8 | reduce | flops 1835008 | bytes 4718594 | tf_op jit(solution)/shard_map/reduce_sum | solution.py:25
  161.6 22.5 %all_to_all.26 = bf16[32,2,2,2048]{3,2,1,0:T(2,128)(2,1)S(1)} all-to-all(bf16[32,2,2,2048]{3,2,1,0:T(2,128)(2,1)S(1)} %copy.52), channel_id=1, replica_groups=mesh['ep_0'=8,'ep_1'=4,'tp'=8] {'ep_0','ep_1'}, dimensions={0} | all-to-all | bytes 1048576 | tf_op jit(solution)/shard_map/all_to_all | solution.py:117
  184.1 1.7 broadcast_in_dim.17
  185.8 6.8 %all-to-all-start.4 = ((bf16[8,16,2048]{2,1,0:T(8,128)(2,1)}), bf16[8,16,2048]{2,1,0:T(8,128)(2,1)S(1)}, u32[]{:S(2)}, u32[]{:S(2)}) async-start(bf16[8,16,2048]{2,1,0:T(8,128)(2,1)} %broadcast_in_dim.17), calls=%async_computation.6 | async-start | bytes 1048576 | tf_op jit(solution)/shard_map/all_to_all | solution.py:18
  193.2 8.8 %all-to-all-done.4 = bf16[8,16,2048]{2,1,0:T(8,128)(2,1)S(1)} async-done(((bf16[8,16,2048]{2,1,0:T(8,128)(2,1)}), bf16[8,16,2048]{2,1,0:T(8,128)(2,1)S(1)}, u32[]{:S(2)}, u32[]{:S(2)}) %all-to-all-start.4) | async-done | bytes 524320 | tf_op jit(solution)/shard_map/all_to_all | solution.py:18
  (93 shorter events, 8.3 us)
Async XLA Ops:
  7.2 91.8 %copy-start = (bf16[2,64,2048]{2,1,0:T(8,128)(2,1)S(1)}, bf16[2,64,2048]{2,1,0:T(8,128)(2,1)}, u32[]{:S(2)}) copy-start(bf16[2,64,2048]{2,1,0:T(8,128)(2,1)} %param.37) | copy-start | bytes 1572868
  7.2 5.0 %copy-start.4 = (f32[16,1,128,128]{3,2,1,0:T(8,128)S(1)}, f32[16,1,128,128]{3,2,1,0:T(8,128)}, u32[]{:S(2)}) copy-start(f32[16,1,128,128]{3,2,1,0:T(8,128)} %param.25) | copy-start | bytes 3145732
  7.2 83.9 %all-gather.2.cloned.1.call-start = ((), (), s32[]{:S(2)}) async-start(), calls=%async_computation.7 | async-start | bytes 2359296 | tf_op jit(solution)/shard_map/all_gather | solution.py:31
  9.9 4.0 %copy-start.3 = (bf16[16,2048]{1,0:T(8,128)(2,1)S(1)}, bf16[16,2048]{1,0:T(8,128)(2,1)}, u32[]{:S(2)}) copy-start(bf16[16,2048]{1,0:T(8,128)(2,1)} %param.23) | copy-start | bytes 196612
  9.9 4.0 %copy-start.5 = (bf16[128,2048]{1,0:T(8,128)(2,1)S(1)}, bf16[128,2048]{1,0:T(8,128)(2,1)}, u32[]{:S(2)}) copy-start(bf16[128,2048]{1,0:T(8,128)(2,1)} %param.31) | copy-start | bytes 1572868
  9.9 4.0 %copy-start.18 = (f32[128]{0:T(128)S(1)}, f32[128]{0:T(128)}, u32[]{:S(2)}) copy-start(f32[128]{0:T(128)} %param.30) | copy-start | bytes 1540
  12.6 18.0 %copy-start.2 = (f32[16,1,128,128]{3,2,1,0:T(8,128)}, f32[16,1,128,128]{3,2,1,0:T(8,128)S(1)}, u32[]{:S(2)}) copy-start(f32[16,1,128,128]{3,2,1,0:T(8,128)S(1)} %multiply_add_fusion) | copy-start | bytes 3145732
  13.6 17.4 %copy-start.13 = (f32[2048]{0:T(1024)S(1)}, f32[2048]{0:T(1024)}, u32[]{:S(2)}) copy-start(f32[2048]{0:T(1024)} %param.32) | copy-start | bytes 24580
  13.9 28.1 %copy-start.16 = (s32[16,6]{0,1:T(8,128)S(1)}, s32[16,6]{0,1:T(8,128)}, u32[]{:S(2)}) copy-start(s32[16,6]{0,1:T(8,128)} %param.33) | copy-start | bytes 1156
  13.9 28.3 %copy-start.17 = (bf16[2048]{0:T(1024)(128)(2,1)S(1)}, bf16[2048]{0:T(1024)(128)(2,1)}, u32[]{:S(2)}) copy-start(bf16[2048]{0:T(1024)(128)(2,1)} %param.41) | copy-start | bytes 12292
  42.7 11.7 %copy-start.7 = (bf16[2048,64]{0,1:T(8,128)(2,1)S(1)}, bf16[2048,64]{0,1:T(8,128)(2,1)}, u32[]{:S(2)}) copy-start(bf16[2048,64]{0,1:T(8,128)(2,1)} %param.38) | copy-start | bytes 786436
  42.7 11.9 %copy-start.8 = (bf16[2048,64]{0,1:T(8,128)(2,1)S(1)}, bf16[2048,64]{0,1:T(8,128)(2,1)}, u32[]{:S(2)}) copy-start(bf16[2048,64]{0,1:T(8,128)(2,1)} %param.39) | copy-start | bytes 786436
  44.3 49.1 %copy-start.10 = (bf16[2048,32]{0,1:T(8,128)(2,1)S(1)}, bf16[2048,32]{0,1:T(8,128)(2,1)}, u32[]{:S(2)}) copy-start(bf16[2048,32]{0,1:T(8,128)(2,1)} %param.42) | copy-start | bytes 393220
  44.3 53.1 %all-to-all-start.1 = ((bf16[32,2,2,2048]{3,2,1,0:T(2,128)(2,1)}), bf16[32,2,2,2048]{3,2,1,0:T(2,128)(2,1)S(1)}, u32[]{:S(2)}, u32[]{:S(2)}) async-start(bf16[32,2,2,2048]{3,2,1,0:T(2,128)(2,1)} %reshape.238), calls=%async_computation.1 | async-start | bytes 1048576 | tf_op jit(solution)/shard_map/all_to_all | solution.py:109
  54.4 74.7 %reduce-scatter.3.cloned.1.call-start = ((), (), s32[]{:S(2)}) async-start(), calls=%async_computation.8 | async-start | bytes 2621440 | tf_op jit(solution)/shard_map/reduce_scatter | solution.py:41
  91.0 2.4 %copy-start.1 = (bf16[512,2048]{1,0:T(8,128)(2,1)S(1)}, bf16[512,2048]{1,0:T(8,128)(2,1)}, u32[]{:S(2)}) copy-start(bf16[512,2048]{1,0:T(8,128)(2,1)} %all-gather.2.cloned.1.call-done) | copy-start | bytes 6291460
  91.0 3.2 %copy-start.11 = (bf16[2048,32]{0,1:T(8,128)(2,1)S(1)}, bf16[2048,32]{0,1:T(8,128)(2,1)}, u32[]{:S(2)}) copy-start(bf16[2048,32]{0,1:T(8,128)(2,1)} %param.43) | copy-start | bytes 393220
  93.5 1.6 copy-start.9
  93.5 1.6 copy-start.12
  102.2 55.8 %all-to-all-start.2 = ((bf16[8,32,2,2,2048]{4,1,3,2,0:T(8,128)(2,1)}), bf16[8,32,2,2,2048]{4,1,3,2,0:T(8,128)(2,1)}, u32[]{:S(2)}, u32[]{:S(2)}) async-start(bf16[8,32,2,2,2048]{4,1,3,2,0:T(8,128)(2,1)} %broadcast_in_dim.14), calls=%async_computation.2 | async-start | bytes 8388608 | tf_op jit(solution)/shard_map/all_to_all | solution.py:18
  109.3 74.8 %reduce-scatter.5.cloned.1.call-start = ((), (), s32[]{:S(2)}) async-start(), calls=%async_computation.9 | async-start | bytes 589824 | tf_op jit(solution)/shard_map/reduce_scatter | solution.py:41
  161.6 31.3 %copy-start.15 = (f32[16,6]{0,1:T(8,128)S(1)}, f32[16,6]{0,1:T(8,128)}, u32[]{:S(2)}) copy-start(f32[16,6]{0,1:T(8,128)} %param.34) | copy-start | bytes 1156
  185.8 16.7 %copy-start.14 = (f32[2048]{0:T(1024)S(1)}, f32[2048]{0:T(1024)}, u32[]{:S(2)}) copy-start(f32[2048]{0:T(1024)} %param.45) | copy-start | bytes 24580
  185.8 16.2 %all-to-all-start.4 = ((bf16[8,16,2048]{2,1,0:T(8,128)(2,1)}), bf16[8,16,2048]{2,1,0:T(8,128)(2,1)S(1)}, u32[]{:S(2)}, u32[]{:S(2)}) async-start(bf16[8,16,2048]{2,1,0:T(8,128)(2,1)} %broadcast_in_dim.17), calls=%async_computation.6 | async-start | bytes 1048576 | tf_op jit(solution)/shard_map/all_to_all | solution.py:18
  (2 other events, 2.6 us)
Sparse Core Ops, SparseCore 0:
  42.1 48.8 all-gather.1
  97.6 31.4 reduce-scatter.2
  131.6 33.6 reduce-scatter.4
where the time goes:
time: 210 us
  waiting for transfers between devices  93.8 us (45%)
  blocking collectives  48.5 us (23%)
  starting transfers between devices  24 us (11%)
  between operations  14.3 us (7%)
  matrix products  13 us (6%)
  local copies, waits for them, and re-layouts  9.35 us (4%)
  other arithmetic  6.77 us (3%)
    all_to_all x2, waiting for transfers between devices, sent_to_all(): lax.all_to_all(jnp.broadcast_to(shard[None], (devices, *shard.shape)), ax...  37.8 us
    all_gather x1, waiting for transfers between devices, gather_axes(): result = lax.all_gather(result, axes[number], axis=dim, tiled=True)  36.2 us
    all_to_all x1, blocking collectives, route_experts(): lax.all_to_all(summed, EP, split_axis=0, concat_axis=0, tiled=True)  22.5 us
    reduce_scatter x2, waiting for transfers between devices, reduced_to_own(): pieces = lax.psum_scatter(pieces, axes[k], scatter_dimension=0, tiled=True)  19.8 us
    all_to_all x1, blocking collectives, sent_to_all(): lax.all_to_all(jnp.broadcast_to(shard[None], (devices, *shard.shape)), ax...  15.1 us
    all_to_all x2, starting transfers between devices, sent_to_all(): lax.all_to_all(jnp.broadcast_to(shard[None], (devices, *shard.shape)), ax...  13.9 us
    all_gather x1, blocking collectives, gather_axes(): result = lax.all_gather(result, axes[number], axis=dim, tiled=True)  10.9 us
    all_to_all x1, starting transfers between devices, route_experts(): lax.all_to_all(outgoing, EP, split_axis=0, concat_axis=0, tiled=True)  10.1 us
  transfers between devices with their start and end apart: 6, of which 4 were waited for; matrix products, arithmetic and copies ran while one was open for 8% of the time, Pallas kernels for 0%

commit v1 on v0

v1 whole, which is shorter than its diff:
```python
import functools

import jax
import jax.numpy as jnp
import numpy as np
from jax import lax
from jax.experimental import pallas as pl
from jax.experimental.pallas import tpu as pltpu
from jax.sharding import PartitionSpec as P

MESH = pl.DeviceIdType.MESH
NX, NY, NZ = 4, 4, 8
D = 2048
HD = 128
HEADS = 8
ROWS = 16
HALF = 8
QUARTER = D // NY
PART = QUARTER // 2
BLOCK = NZ * HALF
TOTAL = NX * BLOCK
NORM_EPS = 1e-05
SCALE = 2.0**0.5
BF16, F32 = jnp.bfloat16, jnp.float32
NT = (((1,), (1,)), ((), ()))
DECAYS = 1.0 - np.exp2(-2.0 - 10.0 * np.arange(HEADS) / (HEADS - 1))
FREQUENCY = (1.0 / 10000.0 ** (np.arange(HD // 2) * 2.0 / HD)).astype(np.float32)


def normed(rows, gain):
    centered = rows - jnp.mean(rows, axis=-1, keepdims=True)
    variance = jnp.mean(centered * centered, axis=-1, keepdims=True)
    return centered * lax.rsqrt(variance + NORM_EPS) * gain


def silu(v):
    return v * jax.nn.sigmoid(v)


def kernel(
    lens, tok_h, state_h, wq_h, wk_h, wv_h, wg_h, hgain_h, wo_h, g1_h, ids_h, ew_h, eg_h, eu_h, ed_h,
    sg_h, su_h, sd_h, side_h, dg_h, du_h, dd_h, g2_h, freq_h,
    out_ref, ns_h,
    tok, state, fresh, wm, hgain, wo, g1, g2, ids, ew, side, freq, wc, wd,
    ro, mx, rm, held, x_all, sc, wr, own, hid, pb, rya, rxb, s2a, s2b, r2a, r2b, z3, rz, gathered,
    in_sem, out_sem, send_sem, recv_sem,
):
    ep, tp = lax.axis_index("ep"), lax.axis_index("tp")
    z, x = ep // NX, ep % NX
    y, c = tp // 2, tp % 2
    here = x * NZ + z

    def at(ep_to, tp_to):
        return {"ep": ep_to, "tp": tp_to}

    def tp_peer(r):
        return at(ep, (tp + r) % 8)

    def y_peer(dy):
        return at(ep, (tp + 2 * dy) % 8)

    def x_peer(dx):
        return at(z * NX + (x + dx) % NX, tp)

    def z_peer(dz):
        return at(((z + dz) % NZ) * NX + x, tp)

    partner = at(ep, tp + 1 - 2 * c)
    barrier = pltpu.get_barrier_semaphore()
    peers = (
        [tp_peer(r) for r in range(1, 8)]
        + [x_peer(d) for d in range(1, NX)]
        + [z_peer(d) for d in range(1, NZ)]
    )
    for peer in peers:
        pl.semaphore_signal(barrier, inc=1, device_id=peer, device_id_type=MESH)

    numbers = {"in": 0, "remote": 0}
    sent = []

    def load(src, dst):
        copy = pltpu.make_async_copy(src, dst, in_sem.at[numbers["in"]])
        numbers["in"] += 1
        copy.start()
        return copy

    def send(src, dst, peer):
        n = numbers["remote"]
        numbers["remote"] += 1
        copy = pltpu.make_async_remote_copy(
            src_ref=src, dst_ref=dst, send_sem=send_sem.at[n], recv_sem=recv_sem.at[n], device_id=peer,
            device_id_type=MESH,
        )
        copy.start()
        sent.append(copy)
        return copy

    small = [load(ids_h, ids), load(ew_h, ew)]
    first = [load(tok_h, tok)]
    for k, w in enumerate((wq_h, wk_h, wv_h, wg_h)):
        first.append(load(w, wm.at[:, pl.ds(k * HD, HD)]))
    first.append(load(freq_h, freq))
    second = [load(state_h, state), load(hgain_h, hgain), load(wo_h, wo)]
    later = [load(g1_h, g1), load(g2_h, g2), load(side_h, side)]
    pl.semaphore_wait(barrier, len(peers))

    for copy in small:
        copy.wait()
    lane = lax.broadcasted_iota(jnp.int32, (HALF, HD), 1)
    rows_c = pl.ds(pl.multiple_of(c * HALF, HALF), HALF)
    my_ids, my_ew = ids[rows_c, :], ew[rows_c, :]
    table = jnp.zeros((HALF, HD), F32)
    for k in range(6):
        table += jnp.where(lane == my_ids[:, k : k + 1], my_ew[:, k : k + 1], 0.0)
    wr[here] = table
    table_z = [send(wr.at[here], wr.at[here], z_peer(d)) for d in range(1, NZ)]

    arrivals = []
    for src, dst, row, size in (
        (eg_h.at[0], wc, 0, 64), (eg_h.at[1], wc, 128, 64), (eu_h.at[0], wc, 256, 64), (eu_h.at[1], wc, 384, 64),
        (sg_h, wc, 512, 64), (su_h, wc, 640, 64), (dg_h, wc, 768, 32), (du_h, wc, 832, 32),
        (ed_h.at[0], wd, 0, 64), (ed_h.at[1], wd, 128, 64), (sd_h, wd, 256, 64), (dd_h, wd, 384, 32),
    ):
        later.append(load(src, dst.at[pl.ds(row, size), :]))
        arrivals.append(send(src, dst.at[pl.ds(row + size, size), :], partner))
    wd[448:512, :] = jnp.zeros((64, D), BF16)

    for copy in first:
        copy.wait()
    tokens = tok[...].astype(F32).reshape(ROWS, D).astype(BF16)
    projected = jnp.dot(tokens, wm[...], preferred_element_type=F32)
    queries, keys = projected[:, :HD], projected[:, HD : 2 * HD] * HD ** (-0.5)
    values, gating = projected[:, 2 * HD : 3 * HD], projected[:, 3 * HD :]
    row_of = lax.broadcasted_iota(jnp.int32, (ROWS, HD), 0)
    lane_of = lax.broadcasted_iota(jnp.int32, (ROWS, HD), 1)
    position = jnp.zeros((ROWS, HD), jnp.int32)
    for t in range(ROWS):
        position = jnp.where(row_of == t, lens[t], position)
    angles = position.astype(F32) * freq[...]
    cosine = jnp.cos(angles)
    sine = jnp.where(lane_of < HD // 2, -1.0, 1.0) * jnp.sin(angles)
    query_rot = queries * cosine + pltpu.roll(queries, HD // 2, 1) * sine
    key_rot = keys * cosine + pltpu.roll(keys, HD // 2, 1) * sine
    decay = jnp.float32(0.0)
    for h in range(HEADS):
        decay = decay + jnp.where(tp == h, jnp.float32(DECAYS[h]), jnp.float32(0.0))
    q_columns, k_columns = query_rot.T, key_rot.T
    for copy in second:
        copy.wait()
    for t in range(ROWS):
        new = decay * state[t] + k_columns[:, t : t + 1] * values[t : t + 1, :]
        fresh[t] = new
        ro[t : t + 1, :] = jnp.sum(q_columns[:, t : t + 1] * new, axis=0, keepdims=True)
    state_out = pltpu.make_async_copy(fresh, ns_h, out_sem.at[0])
    state_out.start()
    mixed = (normed(ro[...], hgain[...]) * silu(gating)).astype(BF16)
    share = jnp.dot(mixed, wo[...], preferred_element_type=F32)
    mx[...] = share.reshape(2, HALF, D).astype(BF16)

    cols = pl.ds(pl.multiple_of(y * QUARTER, QUARTER), QUARTER)
    shares = []
    for r in range(1, 8):
        to = (tp + r) % 8
        cols_to = pl.ds(pl.multiple_of((to // 2) * QUARTER, QUARTER), QUARTER)
        shares.append(send(mx.at[to % 2, :, cols_to], rm.at[r - 1], tp_peer(r)))
    for copy in table_z:
        copy.wait_recv()
    group = pl.ds(pl.multiple_of(x * NZ, NZ), NZ)
    table_x = [send(wr.at[group], wr.at[group], x_peer(d)) for d in range(1, NX)]
    total = SCALE * tok[c, :, cols].astype(F32) + mx[c, :, cols].astype(F32)
    for r in range(1, 8):
        shares[r - 1].wait_recv()
        total += rm[r - 1].astype(F32)
    held[here, :, cols] = total.astype(BF16)

    gather_z = [send(held.at[here, :, cols], held.at[here, :, cols], z_peer(d)) for d in range(1, NZ)]
    for copy in gather_z:
        copy.wait_recv()
    piece = held.at[group, :, cols]
    by_x, by_y = {}, {}
    for d in (2, 1, 3):
        by_x[d] = send(piece, piece, x_peer(d))
        by_y[d] = send(piece, piece, y_peer(d))
    second_level = []
    for d in (1, 3, 2):
        by_x[d].wait_recv()
        group_d = pl.ds(pl.multiple_of(((x + NX - d) % NX) * NZ, NZ), NZ)
        cols_a = pl.ds(pl.multiple_of(y * QUARTER, PART), PART)
        piece = held.at[group_d, :, cols_a]
        for e in (2, 1, 3):
            second_level.append(send(piece, piece, y_peer(e)))
        by_y[d].wait_recv()
        cols_b = pl.ds(pl.multiple_of(((y + NY - d) % NY) * QUARTER + PART, PART), PART)
        piece = held.at[group, :, cols_b]
        for e in (2, 1, 3):
            second_level.append(send(piece, piece, x_peer(e)))
    for copy in table_x:
        copy.wait_recv()
    for copy in later:
        copy.wait()
    for copy in arrivals:
        copy.wait_recv()
    for copy in second_level:
        copy.wait_recv()

    lanes = lax.broadcasted_iota(jnp.int32, (ROWS, HD), 1)

    def norm_step(i, carry):
        rows = held[pl.ds(2 * i, 2)].astype(F32).reshape(ROWS, D)
        after = normed(rows, g1[...]).astype(BF16)
        x_all[pl.ds(pl.multiple_of(i * ROWS, ROWS), ROWS), :] = after
        switch = jax.nn.sigmoid(jnp.sum(after.astype(F32) * side[...], axis=-1, keepdims=True))
        tables = wr[pl.ds(2 * i, 2)].reshape(ROWS, HD)
        w0 = jnp.sum(jnp.where(lanes == 2 * ep, tables, 0.0), axis=-1, keepdims=True)
        w1 = jnp.sum(jnp.where(lanes == 2 * ep + 1, tables, 0.0), axis=-1, keepdims=True)
        sc[pl.ds(pl.multiple_of(i * ROWS, ROWS), ROWS), :] = jnp.where(
            lanes == 0, w0, jnp.where(lanes == 1, w1, switch)
        )
        return carry

    lax.fori_loop(0, TOTAL // ROWS, norm_step, 0)
    own[...] = normed(held[here].astype(F32), g1[...])

    gates = lax.dot_general(x_all[...], wc[0:256, :], NT, preferred_element_type=F32)
    ups = lax.dot_general(x_all[...], wc[256:512, :], NT, preferred_element_type=F32)
    for e in range(2):
        lo, hi = e * HD, (e + 1) * HD
        hid[:, lo:hi] = (silu(gates[:, lo:hi]) * ups[:, lo:hi] * sc[:, e : e + 1]).astype(BF16)
    both = lax.dot_general(x_all[...], wc[512:768, :], NT, preferred_element_type=F32)
    block_of = lax.broadcasted_iota(jnp.int32, (TOTAL, HD), 0) // HALF
    shared = jnp.where(block_of == here, silu(both[:, :HD]) * both[:, HD:], 0.0)
    hid[:, 256:384] = shared.astype(BF16)
    wide = lax.dot_general(x_all[...], wc[768:896, :], NT, preferred_element_type=F32)
    wide_lane = lax.broadcasted_iota(jnp.int32, (TOTAL, HD), 1)
    dense = silu(wide) * pltpu.roll(wide, HD // 2, 1) * sc[:, 2:3]
    hid[:, 384:512] = jnp.where(wide_lane < HD // 2, dense, 0.0).astype(BF16)

    def rows_of(dx):
        return pl.ds(pl.multiple_of(((x + dx) % NX) * BLOCK, BLOCK), BLOCK)

    first_a, first_b = {}, {}
    for dy in (2, 1, 3, 0):
        base = ((y + dy) % NY) * QUARTER
        pair = pl.ds(pl.multiple_of(base, QUARTER), QUARTER)
        product = jnp.dot(hid[...], wd[:, pair], preferred_element_type=F32)
        pb[:, pair] = product.astype(BF16)
        for dx in (2, 1, 3, 0):
            if dy:
                piece = pb.at[rows_of(dx), pl.ds(pl.multiple_of(base, PART), PART)]
                first_a[dx, dy] = send(piece, rya.at[dy - 1, dx], y_peer(dy))
            if dx:
                piece = pb.at[rows_of(dx), pl.ds(pl.multiple_of(base + PART, PART), PART)]
                first_b[dx, dy] = send(piece, rxb.at[dx - 1, dy], x_peer(dx))
    second_a, second_b = {}, {}
    for d in (2, 1, 3, 0):
        part_a = pb[rows_of(d), pl.ds(pl.multiple_of(y * QUARTER, PART), PART)].astype(F32)
        for e in (1, 3, 2):
            first_a[d, e].wait_recv()
            part_a += rya[e - 1, d].astype(F32)
        if d:
            s2a[d - 1] = part_a.astype(BF16)
            second_a[d] = send(s2a.at[d - 1], r2a.at[d - 1], x_peer(d))
        cols_b = pl.ds(pl.multiple_of(((y + d) % NY) * QUARTER + PART, PART), PART)
        part_b = pb[rows_of(0), cols_b].astype(F32)
        for e in (1, 3, 2):
            first_b[e, d].wait_recv()
            part_b += rxb[e - 1, d].astype(F32)
        if d:
            s2b[d - 1] = part_b.astype(BF16)
            second_b[d] = send(s2b.at[d - 1], r2b.at[d - 1], y_peer(d))
    for d in (1, 3, 2):
        second_a[d].wait_recv()
        part_a += r2a[d - 1].astype(F32)
        second_b[d].wait_recv()
        part_b += r2b[d - 1].astype(F32)
    z3[:, :, :PART] = part_a.reshape(NZ, HALF, PART).astype(BF16)
    z3[:, :, PART:] = part_b.reshape(NZ, HALF, PART).astype(BF16)
    last = [send(z3.at[(z + d) % NZ], rz.at[d - 1], z_peer(d)) for d in range(1, NZ)]
    total = SCALE * own[:, cols].astype(BF16).astype(F32) + z3[z].astype(F32)
    for d in range(1, NZ):
        last[d - 1].wait_recv()
        total += rz[d - 1].astype(F32)
    gathered[c, :, cols] = total.astype(BF16)
    finals = [send(gathered.at[c, :, cols], gathered.at[c, :, cols], tp_peer(r)) for r in range(1, 8)]
    for copy in finals:
        copy.wait_recv()
    out_ref[...] = normed(gathered[...].astype(F32).reshape(ROWS, D), g2[...]).astype(BF16)
    for copy in sent:
        copy.wait_send()
    state_out.wait()


def per_device(
    tokens, lengths, old_state, query_weight, key_weight, value_weight, gate_weight, head_gain, output_weight,
    first_gain, expert_ids, expert_weights, expert_gate, expert_up, expert_down, shared_gate, shared_up,
    shared_down, side_gate, dense_gate, dense_up, dense_down, second_gain,
):
    frequency = jnp.asarray(np.concatenate([FREQUENCY, FREQUENCY])[None, :])
    anywhere = pl.BlockSpec(memory_space=pl.ANY)
    vmem = pltpu.VMEM
    out, fresh = pl.pallas_call(
        kernel,
        out_shape=(
            jax.ShapeDtypeStruct((ROWS, D), BF16),
            jax.ShapeDtypeStruct((ROWS, HD, HD), F32),
        ),
        in_specs=[pl.BlockSpec(memory_space=pltpu.SMEM)] + [anywhere] * 23,
        out_specs=(pl.BlockSpec(memory_space=pltpu.VMEM), anywhere),
        scratch_shapes=[
            vmem((2, HALF, D), BF16),
            vmem((ROWS, HD, HD), F32),
            vmem((ROWS, HD, HD), F32),
            vmem((D, 4 * HD), BF16),
            vmem((1, HD), F32),
            vmem((HD, D), BF16),
            vmem((1, D), F32),
            vmem((1, D), F32),
            vmem((ROWS, 6), jnp.int32),
            vmem((ROWS, 6), F32),
            vmem((1, D), F32),
            vmem((1, HD), F32),
            vmem((896, D), BF16),
            vmem((512, D), BF16),
            vmem((ROWS, HD), F32),
            vmem((2, HALF, D), BF16),
            vmem((7, HALF, QUARTER), BF16),
            vmem((NX * NZ, HALF, D), BF16),
            vmem((TOTAL, D), BF16),
            vmem((TOTAL, HD), F32),
            vmem((NX * NZ, HALF, HD), F32),
            vmem((HALF, D), F32),
            vmem((TOTAL, 512), BF16),
            vmem((TOTAL, D), BF16),
            vmem((3, 4, BLOCK, PART), BF16),
            vmem((3, 4, BLOCK, PART), BF16),
            vmem((3, BLOCK, PART), BF16),
            vmem((3, BLOCK, PART), BF16),
            vmem((3, BLOCK, PART), BF16),
            vmem((3, BLOCK, PART), BF16),
            vmem((NZ, HALF, QUARTER), BF16),
            vmem((7, HALF, QUARTER), BF16),
            vmem((2, HALF, D), BF16),
            pltpu.SemaphoreType.DMA((26,)),
            pltpu.SemaphoreType.DMA((1,)),
            pltpu.SemaphoreType.DMA((106,)),
            pltpu.SemaphoreType.DMA((106,)),
        ],
        compiler_params=pltpu.CompilerParams(
            collective_id=0, has_side_effects=True, vmem_limit_bytes=60 * 1024 * 1024
        ),
    )(
        lengths,
        tokens.reshape(2, HALF, D),
        old_state.reshape(ROWS, HD, HD),
        query_weight,
        key_weight,
        value_weight,
        gate_weight,
        head_gain.reshape(1, HD),
        output_weight,
        first_gain.reshape(1, D),
        expert_ids,
        expert_weights,
        expert_gate.transpose(0, 2, 1),
        expert_up.transpose(0, 2, 1),
        expert_down,
        shared_gate.T,
        shared_up.T,
        shared_down,
        side_gate.astype(F32).reshape(1, D),
        dense_gate.T,
        dense_up.T,
        dense_down,
        second_gain.reshape(1, D),
        frequency,
    )
    return out, fresh.reshape(ROWS, 1, HD, HD)


def solution(mesh):
    return jax.shard_map(
        per_device,
        mesh=mesh,
        in_specs=(
            P("ep", None), P("ep"), P("ep", "tp", None, None),
            P(None, "tp"), P(None, "tp"), P(None, "tp"), P(None, "tp"),
            P("tp"), P("tp", None), P(), P("ep", None), P("ep", None),
            P("ep", None, "tp"), P("ep", None, "tp"), P("ep", "tp", None),
            P(None, "tp"), P(None, "tp"), P("tp", None), P(),
            P(None, ("ep", "tp")), P(None, ("ep", "tp")), P(("ep", "tp"), None), P(),
        ),
        out_specs=(P("ep", None), P("ep", "tp", None, None)),
        check_vma=False,
    )
```

time: 210 us -> 69.5 us (0.33)
  waiting for transfers between devices: 93.8 us -> 0 us
  Pallas kernels: 0 us -> 62.1 us
  blocking collectives: 48.5 us -> 0 us
  starting transfers between devices: 24 us -> 0 us
  between operations: 14.3 us -> 0.65 us
  matrix products: 13 us -> 0 us
  other arithmetic: 6.77 us -> 0.59 us
  local copies, waits for them, and re-layouts: 9.35 us -> 5.82 us
    pallas_call x0 -> x1, Pallas kernels: none -> 62.1 us  [per_device(): pl.pallas_call(kernel, out_shape=(jax.ShapeDtypeStruct((ROWS, D), BF16),...]
    all_to_all x3 -> x0, waiting for transfers between devices: 37.8 us -> none  [the longest x2 37.8 us: sent_to_all(): lax.all_to_all(jnp.broadcast_to(shard[None], (devices, *shard.shape)), ax...]
    all_to_all x2 -> x0, blocking collectives: 37.5 us -> none  [the longest x1 22.5 us: route_experts(): lax.all_to_all(summed, EP, split_axis=0, concat_axis=0, tiled=True)]
    all_gather x1 -> x0, waiting for transfers between devices: 36.2 us -> none  [gather_axes(): result = lax.all_gather(result, axes[number], axis=dim, tiled=True)]
    all_to_all x3 -> x0, starting transfers between devices: 23.9 us -> none  [the longest x2 13.9 us: sent_to_all(): lax.all_to_all(jnp.broadcast_to(shard[None], (devices, *shard.shape)), ax...]
    reduce_scatter x2 -> x0, waiting for transfers between devices: 19.8 us -> none  [reduced_to_own(): pieces = lax.psum_scatter(pieces, axes[k], scatter_dimension=0, tiled=True)]
    dot_general x15 -> x0, matrix products: 13 us -> none  [the longest x1 2.38 us: side_branch(): jnp.dot(row_piece, side_gate, preferred_element_type=jnp.float32)]
    all_gather x1 -> x0, blocking collectives: 10.9 us -> none  [gather_axes(): result = lax.all_gather(result, axes[number], axis=dim, tiled=True)]
  transfers between devices with their start and end apart: 6 -> 0, of which waited for: 4 -> 0; matrix products, arithmetic and copies ran while one was open for 8% -> 0% of each run, Pallas kernels for 0% -> 0%
where the time goes in v1:
time: 69.5 us; the launch traced here: 69.2 us
  Pallas kernels  62.1 us (89%)
  local copies, waits for them, and re-layouts  5.82 us (8%)
    pallas_call x1, Pallas kernels, per_device(): pl.pallas_call(kernel, out_shape=(jax.ShapeDtypeStruct((ROWS, D), BF16),...  62.1 us
    unnamed x10, local copies, waits for them, and re-layouts  5.82 us

profile of v1, /device:TPU:1, one launch (start us, length us, event | category | flops | bytes accessed | tf_op | source)
XLA Modules:
  0.0 69.2 jit_solution(5003696934012770667)
XLA Ops:
  0.6 0.0 copy-start
  0.6 0.7 copy-done
  1.3 0.0 copy-start.1
  1.3 0.7 copy.26.ids_h
  2.0 0.0 copy-done.1
  2.0 0.0 copy-start.2
  2.0 0.7 copy.27.ew_h
  2.7 0.0 copy-done.2
  2.7 0.6 reshape.35
  3.3 62.1 %shard_map.239 = (bf16[16,2048]{1,0:T(8,128)(2,1)}, f32[16,128,128]{2,1,0:T(8,128)}) custom-call(s32[16]{0:T(128)} %lens.1, bf16[2,8,2048]{2,1,0:T(8,128)(2,1)} %bitcast.23, f32[16,128,128]{2,1,0:T(8,128)} %bitcast.16, bf16[2048,128]{1,0:T(8,128)(2,1)} %wq_h.1, bf16[2048,128]{1,0:T(8,128)(2,1)} %wk_h.1, bf16[2048,128]{1,0:T(8,128)(2,1)} %wv_h.1, ...), custom_call_target="tpu_custom_call" | custom-call | tf_op jit(solution)/shard_map/pallas_call | solution.py:301
  65.4 1.5 %copy.31 = bf16[16,2048]{1,0:T(8,128)(2,1)} copy(bf16[16,2048]{1,0:T(8,128)(2,1)} %get-tuple-element.10) | data formatting | bytes 131072
  66.9 2.3 %copy.32 = f32[16,1,128,128]{3,2,1,0:T(8,128)} copy(f32[16,1,128,128]{3,2,1,0:T(8,128)} %bitcast.15) | data formatting | bytes 2097152
Async XLA Ops:
  0.6 0.7 copy-start
  1.3 0.7 copy-start.1
  2.0 0.7 copy-start.2
